TPU v7x, 32 devices: a whole 2x2x4 slice. The times are simulated.
32 devices in a mesh: ep: 8 (over z, core), tp: 4 (over y, x).
Axes of the slice: x: 2, y: 2, z: 4, core: 2. Of those that a mesh axis runs over, the one named last changes fastest.
Arguments:
- tokens: bfloat16 [2048, 2048], P('ep'), may hold values from -6 to 6
- norm_gain: float32 [2048], replicated, may hold values from 0.1 to 1.9
- route_ids: int32 [2048, 4], P('ep'), may hold values from 0 to 15, all different within a row; in each aligned block of 256 rows (0 to 255, 256 to 511, ...) at most 96 rows name the same one
- route_weights: float32 [2048, 4], P('ep'), may hold values from 0.1 to 1
- w_gate: bfloat16 [16, 2048, 2048], P('ep', None, 'tp'), may hold values from -0.33007812 to 0.33007812
- w_up: bfloat16 [16, 2048, 2048], P('ep', None, 'tp'), may hold values from -0.33007812 to 0.33007812
- w_down: bfloat16 [16, 2048, 2048], P('ep', None, 'tp'), may hold values from -0.026489258 to 0.026489258
Outputs:
- mixed_out: bfloat16 [2048, 2048], P('ep', 'tp')
Inputs may be any that keep to these rules, and one draw needn't show every extreme that they name: `route_ids`: each token names 4 different experts. Within the tokens of one index of ep (aligned blocks of 256 tokens) no expert is named more than 96 times, a bound that some block reaches.
All inputs are finite; a program needn't handle non-finite values.
Results may differ from a plain program's by a relative error of at most 0.007.
Values may be sent and summed in bfloat16 or wider, within the bound.
A program may use at most 64 MiB of HBM per device.

v0:
```python
import jax
import jax.numpy as jnp
from jax import lax
from jax.sharding import PartitionSpec as P

swiglu_limit = 7.0
swiglu_alpha = 1.702
norm_eps = 1e-05


def clamped_units(gate_pre, up_pre):
    capped = jnp.minimum(gate_pre, swiglu_limit)
    linear = jnp.clip(up_pre, -swiglu_limit, swiglu_limit)
    return capped * jax.nn.sigmoid(swiglu_alpha * capped) * (linear + 1.0)


def expert_work(outgoing, gate_weight, up_weight, down_weight):
    received = lax.all_to_all(outgoing, "ep", split_axis=1, concat_axis=1, tiled=True)
    local_count, sources, capacity, columns = received.shape
    row_count = sources * capacity
    row_block = received.reshape(local_count, row_count, columns)
    shard_piece = lax.all_gather(row_block, "tp", axis=2, tiled=True)
    gate_sum = jnp.einsum(
        "lrd,ldf->lrf", shard_piece, gate_weight, preferred_element_type=jnp.float32
    )
    up_sum = jnp.einsum("lrd,ldf->lrf", shard_piece, up_weight, preferred_element_type=jnp.float32)
    activation = clamped_units(gate_sum, up_sum).astype(jnp.bfloat16)
    out_cols = down_weight.shape[2]
    result = jnp.einsum(
        "lrf,lfd->lrd",
        lax.all_gather(activation, "tp", axis=2, tiled=True),
        down_weight,
        preferred_element_type=jnp.float32,
    )
    result = result.astype(jnp.bfloat16).reshape(local_count, sources, capacity, out_cols)
    return lax.all_to_all(result, "ep", split_axis=1, concat_axis=1, tiled=True)


def per_device(tokens, norm_gain, route_ids, route_weights, w_gate, w_up, w_down):
    local_count = w_gate.shape[0]
    sources = lax.axis_size("ep")
    tp_count = lax.axis_size("tp")
    width = tokens.shape[1]
    columns = width // tp_count
    experts = local_count * sources
    tok_rows, top_count = route_ids.shape
    capacity = 3 * tok_rows * top_count // (2 * experts)
    values = tokens.astype(jnp.float32)
    row_mean = jnp.mean(values, axis=1, keepdims=True)
    centred = values - row_mean
    row_var = jnp.mean(centred * centred, axis=1, keepdims=True)
    offset = lax.axis_index("tp") * columns
    own_cols = lax.dynamic_slice_in_dim(centred, offset, columns, 1)
    own_gain = lax.dynamic_slice_in_dim(norm_gain, offset, columns, 0)
    normed = (own_cols * lax.rsqrt(row_var + norm_eps) * own_gain).astype(jnp.bfloat16)
    flat_ids = route_ids.reshape(-1)
    matches = (flat_ids[:, None] == jnp.arange(experts, dtype=jnp.int32)[None, :]).astype(jnp.int32)
    earlier = jnp.cumsum(matches, axis=0) - matches
    slot_index = jnp.sum(earlier * matches, axis=1)
    position = (
        flat_ids % local_count * (sources * capacity)
        + flat_ids // local_count * capacity
        + slot_index
    )
    buffer_rows = local_count * sources * capacity
    placed = (
        position.reshape(tok_rows, top_count)[:, :, None]
        == jnp.arange(buffer_rows, dtype=jnp.int32)[None, None, :]
    )
    placement_matrix = jnp.any(placed, axis=1).astype(jnp.bfloat16)
    outgoing = jnp.einsum("tp,td->pd", placement_matrix, normed, preferred_element_type=jnp.float32)
    outgoing = outgoing.astype(jnp.bfloat16).reshape(local_count, sources, capacity, columns)
    returned = jnp.concatenate(
        [
            expert_work(
                outgoing[number : number + 1],
                w_gate[number : number + 1],
                w_up[number : number + 1],
                w_down[number : number + 1],
            )
            for number in range(local_count)
        ],
        axis=0,
    )
    flat_out = returned.reshape(buffer_rows, columns)
    picked = flat_out[position].reshape(tok_rows, top_count, columns).astype(jnp.float32)
    return jnp.sum(picked * route_weights[:, :, None], axis=1).astype(jnp.bfloat16)


def solution(mesh):
    return jax.shard_map(
        per_device,
        mesh=mesh,
        in_specs=(
            P("ep", None),
            P(),
            P("ep", None),
            P("ep", None),
            P("ep", None, "tp"),
            P("ep", None, "tp"),
            P("ep", None, "tp"),
        ),
        out_specs=P("ep", "tp"),
        check_vma=False,
    )
```

profile of v0, /device:TPU:0, one launch (start us, length us, event | category | flops | bytes accessed | tf_op | source)
XLA Modules:
  0.0 269.5 jit_solution(14024327743090888040)
XLA Ops:
  6.5 0.0 copy-start
  6.5 0.0 all-gather.7.cloned.1.call-start
  6.5 0.9 copy.62
  7.4 0.1 eq.44
  7.6 0.1 eq.40
  7.7 4.5 %reduce-window.6 = s32[16,8,128]{2,1,0:T(8,128)S(1)} reduce-window(s32[16,8,128]{2,1,0:T(8,128)S(1)} %fusion.42, s32[]{:T(128)} %constant.28.clone.1), window={size=1x1x128 pad=0_0x0_0x127_0}, to_apply=%region_0.0 | reduce-window | flops 2080768 | bytes 131076 | tf_op jit(solution)/shard_map/reduce-window
  12.2 0.1 slice.50
  12.3 0.1 copy.64
  12.5 0.1 copy.65
  12.5 0.1 broadcast_add_fusion
  12.7 0.1 reduce_sum.41
  12.8 0.1 copy.66
  12.9 0.7 fusion.45
  13.6 1.7 fusion
  15.3 0.0 copy-done
  15.3 0.2 convert_reduce_fusion
  15.6 0.4 multiply_reduce_fusion.1
  16.0 0.8 dynamic_slice.7
  16.8 1.7 convolution_convert_fusion
  18.5 0.1 fusion.53
  18.6 27.2 %all_to_all.20 = bf16[1,8,96,512]{3,2,0,1:T(8,128)(2,1)} all-to-all(bf16[1,8,96,512]{3,2,0,1:T(8,128)(2,1)S(1)} %bitcast.82), channel_id=1, replica_groups=mesh['ep'=8,'tp'=4] {'ep'}, dimensions={1} | all-to-all | bytes 1572864 | tf_op jit(solution)/shard_map/all_to_all | solution.py:18
  45.8 0.0 all-gather.7.cloned.1.call-update
  45.8 0.0 all-gather.9.cloned.1.call-start
  45.9 24.0 %all_to_all.21 = bf16[1,8,96,512]{3,2,0,1:T(8,128)(2,1)} all-to-all(bf16[1,8,96,512]{3,2,0,1:T(8,128)(2,1)S(1)} %bitcast.81), channel_id=1, replica_groups=mesh['ep'=8,'tp'=4] {'ep'}, dimensions={1} | all-to-all | bytes 1572864 | tf_op jit(solution)/shard_map/all_to_all | solution.py:18
  69.9 0.0 all-gather.9.cloned.1.call-update
  69.9 0.0 all-gather.11.cloned.1.call-start
  70.0 18.6 %all-gather.7.cloned.1.call-done = bf16[1,768,2048]{2,1,0:T(8,128)(2,1)} async-done(((bf16[1,768,512]{2,1,0:T(8,128)(2,1)}), bf16[1,768,2048]{2,1,0:T(8,128)(2,1)}) %all-gather.7.cloned.1.call-update) | async-done | bytes 3145744 | tf_op jit(solution)/shard_map/all_gather | solution.py:22
  88.6 0.0 copy-start.2
  88.6 0.0 copy-start.5
  88.6 4.5 %fusion.7 = f32[768,512]{1,0:T(8,128)S(1)} fusion(bf16[1,768,2048]{2,1,0:T(8,128)(2,1)} %all-gather.7.cloned.1.call-done, bf16[2,2048,512]{2,1,0:T(8,128)(2,1)} %param.11), kind=kOutput, calls=%fused_computation.9 | convolution fusion | flops 1610612736 | bytes 6815744 | tf_op jit(solution)/shard_map/lrd,ldf->lrf/dot_general | solution.py:23
  93.1 0.0 copy-done.2
  93.1 0.2 copy-done.5
  93.3 3.0 %multiply_convert_fusion.1 = bf16[768,512]{1,0:T(8,128)(2,1)} fusion(f32[768,512]{1,0:T(8,128)S(1)} %fusion.7, bf16[2,2048,512]{2,1,0:T(8,128)(2,1)S(1)} %copy-done.2, bf16[1,768,2048]{2,1,0:T(8,128)(2,1)S(1)} %copy-done.5), kind=kOutput, calls=%fused_computation.32 | convolution fusion | flops 1614544896 | bytes 7602176 | tf_op jit(solution)/shard_map/lrd,ldf->lrf/dot_general | solution.py:26
  96.3 0.0 all-gather.11.cloned.1.call-update
  96.4 0.0 all-gather.13.cloned.1.call-start
  96.4 37.8 %all-gather.9.cloned.1.call-done = bf16[1,768,2048]{2,1,0:T(8,128)(2,1)} async-done(((bf16[1,768,512]{2,1,0:T(8,128)(2,1)}), bf16[1,768,2048]{2,1,0:T(8,128)(2,1)}) %all-gather.9.cloned.1.call-update) | async-done | bytes 3145744 | tf_op jit(solution)/shard_map/all_gather | solution.py:22
  134.2 0.0 copy-start.3
  134.2 0.0 copy-start.4
  134.2 4.5 %fusion.3 = f32[768,512]{1,0:T(8,128)S(1)} fusion(bf16[1,768,2048]{2,1,0:T(8,128)(2,1)} %all-gather.9.cloned.1.call-done, bf16[2,2048,512]{2,1,0:T(8,128)(2,1)} %param.11), kind=kOutput, calls=%fused_computation.5 | convolution fusion | flops 1610612736 | bytes 6815744 | tf_op jit(solution)/shard_map/lrd,ldf->lrf/dot_general | solution.py:23
  138.7 0.0 copy-done.3
  138.7 0.2 copy-done.4
  138.9 3.0 %multiply_convert_fusion = bf16[768,512]{1,0:T(8,128)(2,1)} fusion(f32[768,512]{1,0:T(8,128)S(1)} %fusion.3, bf16[2,2048,512]{2,1,0:T(8,128)(2,1)S(1)} %copy-done.3, bf16[1,768,2048]{2,1,0:T(8,128)(2,1)S(1)} %copy-done.4), kind=kOutput, calls=%fused_computation.31 | convolution fusion | flops 1614544896 | bytes 7602176 | tf_op jit(solution)/shard_map/lrd,ldf->lrf/dot_general | solution.py:26
  141.9 0.0 all-gather.13.cloned.1.call-update
  141.9 37.8 %all-gather.11.cloned.1.call-done = bf16[768,2048]{1,0:T(8,128)(2,1)} async-done(((bf16[768,512]{1,0:T(8,128)(2,1)}), bf16[768,2048]{1,0:T(8,128)(2,1)}) %all-gather.11.cloned.1.call-update) | async-done | bytes 3145744 | tf_op jit(solution)/shard_map/all_gather | solution.py:31
  179.8 5.2 %fusion.31 = bf16[768,512]{1,0:T(8,128)(2,1)} fusion(bf16[768,2048]{1,0:T(8,128)(2,1)} %all-gather.11.cloned.1.call-done, bf16[2,2048,512]{2,1,0:T(8,128)(2,1)} %param.13), kind=kOutput, calls=%fused_computation.33 | convolution fusion | flops 1611005952 | bytes 6029312 | tf_op jit(solution)/shard_map/lrf,lfd->lrd/dot_general | solution.py:29
  185.0 4.6 %all-to-all-start.1 = ((bf16[1,8,96,512]{3,2,0,1:T(8,128)(2,1)}), bf16[1,8,96,512]{3,2,0,1:T(8,128)(2,1)S(1)}, u32[]{:S(2)}, u32[]{:S(2)}) async-start(bf16[1,8,96,512]{3,2,0,1:T(8,128)(2,1)} %bitcast.10), calls=%async_computation.1 | async-start | bytes 1572864 | tf_op jit(solution)/shard_map/all_to_all | solution.py:36
  189.6 0.0 copy-start.1
  189.6 35.6 %all-gather.13.cloned.1.call-done = bf16[768,2048]{1,0:T(8,128)(2,1)} async-done(((bf16[768,512]{1,0:T(8,128)(2,1)}), bf16[768,2048]{1,0:T(8,128)(2,1)}) %all-gather.13.cloned.1.call-update) | async-done | bytes 3145744 | tf_op jit(solution)/shard_map/all_gather | solution.py:31
  225.2 5.2 %fusion.34 = bf16[768,512]{1,0:T(8,128)(2,1)} fusion(bf16[768,2048]{1,0:T(8,128)(2,1)} %all-gather.13.cloned.1.call-done, bf16[2,2048,512]{2,1,0:T(8,128)(2,1)} %param.13), kind=kOutput, calls=%fused_computation.34 | convolution fusion | flops 1611005952 | bytes 6029312 | tf_op jit(solution)/shard_map/lrf,lfd->lrd/dot_general | solution.py:29
  230.4 0.0 all-to-all-done.1
  230.4 4.6 %all-to-all-start.3 = ((bf16[1,8,96,512]{3,2,0,1:T(8,128)(2,1)}), bf16[1,8,96,512]{3,2,0,1:T(8,128)(2,1)S(1)}, u32[]{:S(2)}, u32[]{:S(2)}) async-start(bf16[1,8,96,512]{3,2,0,1:T(8,128)(2,1)} %bitcast.19), calls=%async_computation.3 | async-start | bytes 1572864 | tf_op jit(solution)/shard_map/all_to_all | solution.py:36
  235.0 0.1 reshape.289
  235.1 0.0 copy-done.1
  235.1 0.1 copy.73
  235.3 20.6 %all-to-all-done.3 = bf16[1,8,96,512]{3,2,0,1:T(8,128)(2,1)S(1)} async-done(((bf16[1,8,96,512]{3,2,0,1:T(8,128)(2,1)}), bf16[1,8,96,512]{3,2,0,1:T(8,128)(2,1)S(1)}, u32[]{:S(2)}, u32[]{:S(2)}) %all-to-all-start.3) | async-done | bytes 786464 | tf_op jit(solution)/shard_map/all_to_all | solution.py:36
  255.9 0.1 pad_maximum_fusion
  256.1 0.1 copy.71
  256.2 4.0 %gather_fusion = bf16[1024,512]{1,0:T(8,128)(2,1)S(1)} fusion(bf16[1536,512]{1,0:T(8,128)(2,1)S(1)} %bitcast.78, s32[1024]{0:T(1024)S(1)} %broadcast_clamp_fusion), kind=kCustom, calls=%fused_computation | custom fusion | bytes 2101248 | tf_op jit(solution)/shard_map/gather | solution.py:86
  260.2 0.7 reshape.290
  260.9 2.1 multiply_reduce_fusion
  (8 shorter events, 0.1 us)
Async XLA Ops:
  6.5 8.8 %copy-start = (bf16[256,2048]{1,0:T(8,128)(2,1)S(1)}, bf16[256,2048]{1,0:T(8,128)(2,1)}, u32[]{:S(2)}) copy-start(bf16[256,2048]{1,0:T(8,128)(2,1)} %param.7) | copy-start | bytes 3145732
  6.5 82.1 %all-gather.7.cloned.1.call-start = ((), (), s32[]{:S(2)}) async-start(), calls=%async_computation.4 | async-start | bytes 3932160 | tf_op jit(solution)/shard_map/all_gather | solution.py:22
  45.8 88.4 %all-gather.9.cloned.1.call-start = ((), (), s32[]{:S(2)}) async-start(), calls=%async_computation.5 | async-start | bytes 3932160 | tf_op jit(solution)/shard_map/all_gather | solution.py:22
  69.9 109.8 %all-gather.11.cloned.1.call-start = ((), (), s32[]{:S(2)}) async-start(), calls=%async_computation.6 | async-start | bytes 3932160 | tf_op jit(solution)/shard_map/all_gather | solution.py:31
  88.6 4.5 %copy-start.2 = (bf16[2,2048,512]{2,1,0:T(8,128)(2,1)S(1)}, bf16[2,2048,512]{2,1,0:T(8,128)(2,1)}, u32[]{:S(2)}) copy-start(bf16[2,2048,512]{2,1,0:T(8,128)(2,1)} %param.12) | copy-start | bytes 12582916
  88.6 4.7 %copy-start.5 = (bf16[1,768,2048]{2,1,0:T(8,128)(2,1)S(1)}, bf16[1,768,2048]{2,1,0:T(8,128)(2,1)}, u32[]{:S(2)}) copy-start(bf16[1,768,2048]{2,1,0:T(8,128)(2,1)} %all-gather.7.cloned.1.call-done) | copy-start | bytes 9437188
  96.4 128.8 %all-gather.13.cloned.1.call-start = ((), (), s32[]{:S(2)}) async-start(), calls=%async_computation.7 | async-start | bytes 3932160 | tf_op jit(solution)/shard_map/all_gather | solution.py:31
  134.2 4.5 %copy-start.3 = (bf16[2,2048,512]{2,1,0:T(8,128)(2,1)S(1)}, bf16[2,2048,512]{2,1,0:T(8,128)(2,1)}, u32[]{:S(2)}) copy-start(bf16[2,2048,512]{2,1,0:T(8,128)(2,1)} %param.12) | copy-start | bytes 12582916
  134.2 4.7 %copy-start.4 = (bf16[1,768,2048]{2,1,0:T(8,128)(2,1)S(1)}, bf16[1,768,2048]{2,1,0:T(8,128)(2,1)}, u32[]{:S(2)}) copy-start(bf16[1,768,2048]{2,1,0:T(8,128)(2,1)} %all-gather.9.cloned.1.call-done) | copy-start | bytes 9437188
  185.0 45.4 %all-to-all-start.1 = ((bf16[1,8,96,512]{3,2,0,1:T(8,128)(2,1)}), bf16[1,8,96,512]{3,2,0,1:T(8,128)(2,1)S(1)}, u32[]{:S(2)}, u32[]{:S(2)}) async-start(bf16[1,8,96,512]{3,2,0,1:T(8,128)(2,1)} %bitcast.10), calls=%async_computation.1 | async-start | bytes 1572864 | tf_op jit(solution)/shard_map/all_to_all | solution.py:36
  189.6 45.5 %copy-start.1 = (f32[256,4]{0,1:T(4,128)S(1)}, f32[256,4]{0,1:T(4,128)}, u32[]{:S(2)}) copy-start(f32[256,4]{0,1:T(4,128)} %param.10) | copy-start | bytes 12292
  230.4 25.6 %all-to-all-start.3 = ((bf16[1,8,96,512]{3,2,0,1:T(8,128)(2,1)}), bf16[1,8,96,512]{3,2,0,1:T(8,128)(2,1)S(1)}, u32[]{:S(2)}, u32[]{:S(2)}) async-start(bf16[1,8,96,512]{3,2,0,1:T(8,128)(2,1)} %bitcast.19), calls=%async_computation.3 | async-start | bytes 1572864 | tf_op jit(solution)/shard_map/all_to_all | solution.py:36
Sparse Core Ops, SparseCore 0:
  45.9 42.6 all-gather.6
  90.4 43.6 all-gather.8
  136.0 43.6 all-gather.10
  181.4 43.6 all-gather.12
where the time goes:
time: 270 us; the launch traced here: 269 us
  waiting for transfers between devices  150 us (56%)
  blocking collectives  51.2 us (19%)
  matrix products  27 us (10%)
  between operations  13.3 us (5%)
  other arithmetic  10 us (4%)
  starting transfers between devices  9.36 us (3%)
  local copies, waits for them, and re-layouts  8.03 us (3%)
    all_gather x2, waiting for transfers between devices, expert_work(): lax.all_gather(activation, 'tp', axis=2, tiled=True)  73.4 us
    all_gather x2, waiting for transfers between devices, expert_work(): shard_piece = lax.all_gather(row_block, 'tp', axis=2, tiled=True)  56.4 us
    all_to_all x2, blocking collectives, expert_work(): lax.all_to_all(outgoing, 'ep', split_axis=1, concat_axis=1, tiled=True)  51.2 us
    all_to_all x2, waiting for transfers between devices, expert_work(): return lax.all_to_all(result, 'ep', split_axis=1, concat_axis=1, tiled=True)  20.6 us
    dot_general x2, matrix products, expert_work(): jnp.einsum('lrf,lfd->lrd', lax.all_gather(activation, 'tp', axis=2, tiled...  10.4 us
    all_to_all x2, starting transfers between devices, expert_work(): return lax.all_to_all(result, 'ep', split_axis=1, concat_axis=1, tiled=True)  9.23 us
    dot_general x2, matrix products, expert_work(): jnp.einsum('lrd,ldf->lrf', shard_piece, gate_weight, preferred_element_ty...  8.95 us
    dot_general x2, matrix products, expert_work(): jnp.einsum('lrd,ldf->lrf', shard_piece, up_weight, preferred_element_type...  5.99 us
  transfers between devices with their start and end apart: 6, of which 5 were waited for; matrix products, arithmetic and copies ran while one was open for 10% of the time, Pallas kernels for 0%

commit v1 on v0

--- a/solution.py
+++ b/solution.py
@@ -2,10 +2,32 @@
 import jax.numpy as jnp
 from jax import lax
 from jax.sharding import PartitionSpec as P
+from jax.lax import axis_index, axis_size, ppermute
 
 swiglu_limit = 7.0
 swiglu_alpha = 1.702
 norm_eps = 1e-05
+
+
+def shapes_convert(inp, local):
+    axis_id = "tp"
+    m_next = axis_size(axis_id)
+    r_now = axis_index(axis_id)
+    local_out, current_block, parts_out = (m_next, r_now, inp.shape[2])
+    by_place = [(k0, (k0 + 1) % local_out) for k0 in range(local_out)]
+    frames = [(k0, (k0 - 1) % local_out) for k0 in range(local_out)]
+    high = local_out // 2
+    field_out = piece_now = inp
+    kept_arr = local(inp, current_block * parts_out)
+    d = 1
+    while d < high + 1:
+        field_out = ppermute(field_out, axis_name=axis_id, perm=by_place)
+        if d < local_out - high:
+            piece_now = ppermute(piece_now, axis_name=axis_id, perm=frames)
+            kept_arr = kept_arr + local(piece_now, (current_block + d) % local_out * parts_out)
+        kept_arr = kept_arr + local(field_out, (current_block - d) % local_out * parts_out)
+        d += 1
+    return kept_arr
 
 
 def clamped_units(gate_pre, up_pre):
@@ -26,11 +48,14 @@
     up_sum = jnp.einsum("lrd,ldf->lrf", shard_piece, up_weight, preferred_element_type=jnp.float32)
     activation = clamped_units(gate_sum, up_sum).astype(jnp.bfloat16)
     out_cols = down_weight.shape[2]
-    result = jnp.einsum(
-        "lrf,lfd->lrd",
-        lax.all_gather(activation, "tp", axis=2, tiled=True),
-        down_weight,
-        preferred_element_type=jnp.float32,
+    result = shapes_convert(
+        activation,
+        lambda part, at: jnp.einsum(
+            "lrf,lfd->lrd",
+            part,
+            lax.dynamic_slice_in_dim(down_weight, at, part.shape[2], axis=1),
+            preferred_element_type=jnp.float32,
+        ),
     )
     result = result.astype(jnp.bfloat16).reshape(local_count, sources, capacity, out_cols)
     return lax.all_to_all(result, "ep", split_axis=1, concat_axis=1, tiled=True)

time: 270 us -> 288 us (1.067)
  starting transfers between devices: 9.36 us -> 17.6 us
  waiting for transfers between devices: 150 us -> 155 us
  local copies, waits for them, and re-layouts: 8.03 us -> 12.1 us
    all_gather x2 -> x0, waiting for transfers between devices: 73.4 us -> none  [expert_work(): lax.all_gather(activation, 'tp', axis=2, tiled=True)]
    ppermute x0 -> x6, waiting for transfers between devices: none -> 60.1 us  [the longest x4 60.1 us: shapes_convert(): field_out = ppermute(field_out, axis_name=axis_id, perm=by_place)]
    all_gather x2, waiting for transfers between devices: 56.4 us -> 74.1 us  [expert_work(): shard_piece = lax.all_gather(row_block, 'tp', axis=2, tiled=True)]
    ppermute x0 -> x6, starting transfers between devices: none -> 8.14 us  [the longest x4 5.2 us: shapes_convert(): field_out = ppermute(field_out, axis_name=axis_id, perm=by_place)]
    slice x2 -> x3, local copies, waits for them, and re-layouts: 0.21 us -> 4.23 us  [the longest x1 4.03 us: per_device(): w_down[number:number + 1]]
    dot_general x2 -> x8, matrix products: 10.4 us -> 12.1 us  [expert_work(): jnp.einsum('lrf,lfd->lrd', part, lax.dynamic_slice_in_dim(down_weight, at...]
  transfers between devices with their start and end apart: 6 -> 10, of which waited for: 5 -> 5; matrix products, arithmetic and copies ran while one was open for 10% -> 11% of each run, Pallas kernels for 0% -> 0%
where the time goes in v1:
time: 288 us; the launch traced here: 287 us
  waiting for transfers between devices  155 us (54%)
  blocking collectives  51.2 us (18%)
  matrix products  27.9 us (10%)
  starting transfers between devices  17.6 us (6%)
  between operations  13.7 us (5%)
  local copies, waits for them, and re-layouts  12.1 us (4%)
  other arithmetic  10 us (3%)
    all_gather x2, waiting for transfers between devices, expert_work(): shard_piece = lax.all_gather(row_block, 'tp', axis=2, tiled=True)  74.1 us
    ppermute x4, waiting for transfers between devices, shapes_convert(): field_out = ppermute(field_out, axis_name=axis_id, perm=by_place)  60.1 us
    all_to_all x2, blocking collectives, expert_work(): lax.all_to_all(outgoing, 'ep', split_axis=1, concat_axis=1, tiled=True)  51.2 us
    all_to_all x2, waiting for transfers between devices, expert_work(): return lax.all_to_all(result, 'ep', split_axis=1, concat_axis=1, tiled=True)  20.6 us
    dot_general x8, matrix products, expert_work(): jnp.einsum('lrf,lfd->lrd', part, lax.dynamic_slice_in_dim(down_weight, at...  12.1 us
    all_to_all x2, starting transfers between devices, expert_work(): return lax.all_to_all(result, 'ep', split_axis=1, concat_axis=1, tiled=True)  9.45 us
    dot_general x2, matrix products, expert_work(): jnp.einsum('lrd,ldf->lrf', shard_piece, gate_weight, preferred_element_ty...  8.93 us
  transfers between devices with their start and end apart: 10, of which 5 were waited for; matrix products, arithmetic and copies ran while one was open for 11% of the time, Pallas kernels for 0%

profile of v1, /device:TPU:0, one launch (start us, length us, event | category | flops | bytes accessed | tf_op | source)
XLA Modules:
  0.0 287.3 jit_solution(413537357020292983)
XLA Ops:
  6.5 0.0 all-gather.3.cloned.1.call-start
  6.5 0.9 copy.62
  7.4 0.1 eq.51
  7.6 0.1 eq.47
  7.7 4.5 %reduce-window.6 = s32[16,8,128]{2,1,0:T(8,128)S(1)} reduce-window(s32[16,8,128]{2,1,0:T(8,128)S(1)} %fusion.58, s32[]{:T(128)} %constant.76.clone.1), window={size=1x1x128 pad=0_0x0_0x127_0}, to_apply=%region_0.0 | reduce-window | flops 2080768 | bytes 131076 | tf_op jit(solution)/shard_map/reduce-window
  12.2 0.1 slice.50
  12.3 0.1 copy.64
  12.5 0.1 copy.65
  12.5 0.1 broadcast_add_fusion
  12.7 0.1 reduce_sum.41
  12.8 0.1 copy.66
  12.9 0.7 fusion.61
  13.6 1.7 fusion
  15.3 0.0 copy-done.1
  15.3 0.2 convert_reduce_fusion
  15.6 0.4 multiply_reduce_fusion.1
  16.0 0.8 dynamic_slice.31
  16.8 1.7 convolution_convert_fusion
  18.5 0.1 fusion.78
  18.6 27.2 %all_to_all.20 = bf16[1,8,96,512]{3,2,0,1:T(8,128)(2,1)} all-to-all(bf16[1,8,96,512]{3,2,0,1:T(8,128)(2,1)S(1)} %bitcast.116), channel_id=1, replica_groups=mesh['ep'=8,'tp'=4] {'ep'}, dimensions={1} | all-to-all | bytes 1572864 | tf_op jit(solution)/shard_map/all_to_all | solution.py:40
  45.8 0.0 all-gather.3.cloned.1.call-update
  45.8 0.0 all-gather.5.cloned.1.call-start
  45.8 24.0 %all_to_all.21 = bf16[1,8,96,512]{3,2,0,1:T(8,128)(2,1)} all-to-all(bf16[1,8,96,512]{3,2,0,1:T(8,128)(2,1)S(1)} %bitcast.115), channel_id=1, replica_groups=mesh['ep'=8,'tp'=4] {'ep'}, dimensions={1} | all-to-all | bytes 1572864 | tf_op jit(solution)/shard_map/all_to_all | solution.py:40
  69.9 0.0 all-gather.5.cloned.1.call-update
  70.0 4.0 %fusion.77 = (bf16[1,2048,512]{2,1,0:T(8,128)(2,1)}, bf16[1,2048,512]{2,1,0:T(8,128)(2,1)S(1)}) fusion(bf16[2,2048,512]{2,1,0:T(8,128)(2,1)} %param.13), kind=kLoop, calls=%fused_computation.101 | loop fusion | bytes 8388608 | tf_op jit(solution)/shard_map/slice | solution.py:104
  74.0 14.6 %all-gather.3.cloned.1.call-done = bf16[1,768,2048]{2,1,0:T(8,128)(2,1)} async-done(((bf16[1,768,512]{2,1,0:T(8,128)(2,1)}), bf16[1,768,2048]{2,1,0:T(8,128)(2,1)}) %all-gather.3.cloned.1.call-update) | async-done | bytes 3145744 | tf_op jit(solution)/shard_map/all_gather | solution.py:44
  88.6 4.5 %fusion.7 = f32[768,512]{1,0:T(8,128)S(1)} fusion(bf16[1,768,2048]{2,1,0:T(8,128)(2,1)} %all-gather.3.cloned.1.call-done, bf16[2,2048,512]{2,1,0:T(8,128)(2,1)} %param.11), kind=kOutput, calls=%fused_computation.9 | convolution fusion | flops 1610612736 | bytes 6815744 | tf_op jit(solution)/shard_map/lrd,ldf->lrf/dot_general | solution.py:45
  93.1 0.3 copy-done.6
  93.3 2.1 multiply_convert_fusion.1
  95.5 1.5 collective-permute-start.1
  97.0 1.5 collective-permute-start
  98.4 59.5 %all-gather.5.cloned.1.call-done = bf16[1,768,2048]{2,1,0:T(8,128)(2,1)} async-done(((bf16[1,768,512]{2,1,0:T(8,128)(2,1)}), bf16[1,768,2048]{2,1,0:T(8,128)(2,1)}) %all-gather.5.cloned.1.call-update) | async-done | bytes 3145744 | tf_op jit(solution)/shard_map/all_gather | solution.py:44
  157.9 4.5 %fusion.3 = f32[768,512]{1,0:T(8,128)S(1)} fusion(bf16[1,768,2048]{2,1,0:T(8,128)(2,1)} %all-gather.5.cloned.1.call-done, bf16[2,2048,512]{2,1,0:T(8,128)(2,1)} %param.11), kind=kOutput, calls=%fused_computation.5 | convolution fusion | flops 1610612736 | bytes 6815744 | tf_op jit(solution)/shard_map/lrd,ldf->lrf/dot_general | solution.py:45
  162.4 0.3 copy-done.5
  162.6 3.0 %multiply_convert_fusion = bf16[768,512]{1,0:T(8,128)(2,1)} fusion(f32[768,512]{1,0:T(8,128)S(1)} %fusion.3, bf16[2,2048,512]{2,1,0:T(8,128)(2,1)S(1)} %copy-done.4, bf16[1,768,2048]{2,1,0:T(8,128)(2,1)S(1)} %copy-done.5), kind=kOutput, calls=%fused_computation.26 | convolution fusion | flops 1614544896 | bytes 7602176 | tf_op jit(solution)/shard_map/lrd,ldf->lrf/dot_general | solution.py:48
  165.6 1.5 collective-permute-start.3
  167.1 0.5 collective-permute-start.4
  167.6 0.0 collective-permute-done.1
  167.7 1.5 collective-permute-start.2
  169.2 0.6 fusion.43
  169.7 1.7 fusion.31
  171.4 0.0 collective-permute-done
  171.4 1.7 fusion.33
  173.2 45.8 %collective-permute-done.2 = bf16[1,768,512]{2,1,0:T(8,128)(2,1)S(1)} collective-permute-done((bf16[1,768,512]{2,1,0:T(8,128)(2,1)}, bf16[1,768,512]{2,1,0:T(8,128)(2,1)S(1)}, u32[]{:S(2)}, u32[]{:S(2)}) %collective-permute-start.2) | collective-permute-done | bytes 786464 | tf_op jit(solution)/shard_map/ppermute | solution.py:24
  218.9 1.6 add_convert_fusion.1
  220.5 4.6 %all-to-all-start.1 = ((bf16[1,8,96,512]{3,2,0,1:T(8,128)(2,1)}), bf16[1,8,96,512]{3,2,0,1:T(8,128)(2,1)S(1)}, u32[]{:S(2)}, u32[]{:S(2)}) async-start(bf16[1,8,96,512]{3,2,0,1:T(8,128)(2,1)} %bitcast.117), calls=%async_computation.1 | async-start | bytes 1572864 | tf_op jit(solution)/shard_map/all_to_all | solution.py:61
  225.1 0.0 collective-permute-done.4
  225.1 1.6 collective-permute-start.5
  226.8 1.7 fusion.38
  228.5 1.7 fusion.26
  230.2 0.0 collective-permute-done.3
  230.2 1.7 fusion.28
  231.9 14.3 %collective-permute-done.5 = bf16[1,768,512]{2,1,0:T(8,128)(2,1)S(1)} collective-permute-done((bf16[1,768,512]{2,1,0:T(8,128)(2,1)}, bf16[1,768,512]{2,1,0:T(8,128)(2,1)S(1)}, u32[]{:S(2)}, u32[]{:S(2)}) %collective-permute-start.5) | collective-permute-done | bytes 786464 | tf_op jit(solution)/shard_map/ppermute | solution.py:24
  246.2 1.5 add_convert_fusion
  247.7 0.0 all-to-all-done.1
  247.7 4.8 %all-to-all-start.3 = ((bf16[1,8,96,512]{3,2,0,1:T(8,128)(2,1)}), bf16[1,8,96,512]{3,2,0,1:T(8,128)(2,1)S(1)}, u32[]{:S(2)}, u32[]{:S(2)}) async-start(bf16[1,8,96,512]{3,2,0,1:T(8,128)(2,1)} %bitcast.118), calls=%async_computation.3 | async-start | bytes 1572864 | tf_op jit(solution)/shard_map/all_to_all | solution.py:61
  252.5 0.1 reshape.345
  252.7 0.1 copy.73
  252.9 20.6 %all-to-all-done.3 = bf16[1,8,96,512]{3,2,0,1:T(8,128)(2,1)S(1)} async-done(((bf16[1,8,96,512]{3,2,0,1:T(8,128)(2,1)}), bf16[1,8,96,512]{3,2,0,1:T(8,128)(2,1)S(1)}, u32[]{:S(2)}, u32[]{:S(2)}) %all-to-all-start.3) | async-done | bytes 786464 | tf_op jit(solution)/shard_map/all_to_all | solution.py:61
  273.5 0.1 pad_maximum_fusion
  273.6 0.1 copy.71
  273.7 4.0 %gather_fusion = bf16[1024,512]{1,0:T(8,128)(2,1)S(1)} fusion(bf16[1536,512]{1,0:T(8,128)(2,1)S(1)} %bitcast.112, s32[1024]{0:T(1024)S(1)} %broadcast_clamp_fusion), kind=kCustom, calls=%fused_computation | custom fusion | bytes 2101248 | tf_op jit(solution)/shard_map/gather | solution.py:111
  277.7 0.7 reshape.346
  278.4 2.1 multiply_reduce_fusion
  (19 shorter events, 0.1 us)
Async XLA Ops:
  6.5 8.8 %copy-start.1 = (bf16[256,2048]{1,0:T(8,128)(2,1)S(1)}, bf16[256,2048]{1,0:T(8,128)(2,1)}, u32[]{:S(2)}) copy-start(bf16[256,2048]{1,0:T(8,128)(2,1)} %param.7) | copy-start | bytes 3145732
  6.5 82.1 %all-gather.3.cloned.1.call-start = ((), (), s32[]{:S(2)}) async-start(), calls=%async_computation.4 | async-start | bytes 3932160 | tf_op jit(solution)/shard_map/all_gather | solution.py:44
  45.8 112.1 %all-gather.5.cloned.1.call-start = ((), (), s32[]{:S(2)}) async-start(), calls=%async_computation.5 | async-start | bytes 3932160 | tf_op jit(solution)/shard_map/all_gather | solution.py:44
  88.6 4.5 %copy-start.3 = (bf16[2,2048,512]{2,1,0:T(8,128)(2,1)S(1)}, bf16[2,2048,512]{2,1,0:T(8,128)(2,1)}, u32[]{:S(2)}) copy-start(bf16[2,2048,512]{2,1,0:T(8,128)(2,1)} %param.12) | copy-start | bytes 12582916
  88.6 4.7 %copy-start.6 = (bf16[1,768,2048]{2,1,0:T(8,128)(2,1)S(1)}, bf16[1,768,2048]{2,1,0:T(8,128)(2,1)}, u32[]{:S(2)}) copy-start(bf16[1,768,2048]{2,1,0:T(8,128)(2,1)} %all-gather.3.cloned.1.call-done) | copy-start | bytes 9437188
  95.5 72.2 %collective-permute-start.1 = (bf16[1,768,512]{2,1,0:T(8,128)(2,1)S(1)}, bf16[1,768,512]{2,1,0:T(8,128)(2,1)}, u32[]{:S(2)}, u32[]{:S(2)}) collective-permute-start(bf16[1,768,512]{2,1,0:T(8,128)(2,1)S(1)} %bitcast.119), channel_id=1, source_target_pairs={{0,1},{1,2},{2,3},{3,0},{4,5},{5,6},{6,7},{7,4},{8,9},{9,10},{10,1... | collective-permute-start | bytes 2359304 | tf_op jit(solution)/shard_map/ppermute | solution.py:24
  97.0 74.5 %collective-permute-start = (bf16[1,768,512]{2,1,0:T(8,128)(2,1)S(1)}, bf16[1,768,512]{2,1,0:T(8,128)(2,1)}, u32[]{:S(2)}, u32[]{:S(2)}) collective-permute-start(bf16[1,768,512]{2,1,0:T(8,128)(2,1)S(1)} %bitcast.120), channel_id=1, source_target_pairs={{0,3},{1,0},{2,1},{3,2},{4,7},{5,4},{6,5},{7,6},{8,11},{9,8},{10,9... | collective-permute-start | bytes 2359304 | tf_op jit(solution)/shard_map/ppermute | solution.py:26
  157.9 4.5 %copy-start.4 = (bf16[2,2048,512]{2,1,0:T(8,128)(2,1)S(1)}, bf16[2,2048,512]{2,1,0:T(8,128)(2,1)}, u32[]{:S(2)}) copy-start(bf16[2,2048,512]{2,1,0:T(8,128)(2,1)} %param.12) | copy-start | bytes 12582916
  157.9 4.7 %copy-start.5 = (bf16[1,768,2048]{2,1,0:T(8,128)(2,1)S(1)}, bf16[1,768,2048]{2,1,0:T(8,128)(2,1)}, u32[]{:S(2)}) copy-start(bf16[1,768,2048]{2,1,0:T(8,128)(2,1)} %all-gather.5.cloned.1.call-done) | copy-start | bytes 9437188
  162.6 6.5 %copy-start = (bf16[1,2048,512]{2,1,0:T(8,128)(2,1)S(1)}, bf16[1,2048,512]{2,1,0:T(8,128)(2,1)}, u32[]{:S(2)}) copy-start(bf16[1,2048,512]{2,1,0:T(8,128)(2,1)} %get-tuple-element.5) | copy-start | bytes 6291460
  165.6 64.6 %collective-permute-start.3 = (bf16[1,768,512]{2,1,0:T(8,128)(2,1)}, bf16[1,768,512]{2,1,0:T(8,128)(2,1)}, u32[]{:S(2)}, u32[]{:S(2)}) collective-permute-start(bf16[1,768,512]{2,1,0:T(8,128)(2,1)} %bitcast.25), channel_id=1, source_target_pairs={{0,3},{1,0},{2,1},{3,2},{4,7},{5,4},{6,5},{7,6},{8,11},{9,8},{10,9... | collective-permute-start | bytes 2359304 | tf_op jit(solution)/shard_map/ppermute | solution.py:26
  167.1 58.0 %collective-permute-start.4 = (bf16[1,768,512]{2,1,0:T(8,128)(2,1)}, bf16[1,768,512]{2,1,0:T(8,128)(2,1)}, u32[]{:S(2)}, u32[]{:S(2)}) collective-permute-start(bf16[1,768,512]{2,1,0:T(8,128)(2,1)} %bitcast.25), channel_id=1, source_target_pairs={{0,1},{1,2},{2,3},{3,0},{4,5},{5,6},{6,7},{7,4},{8,9},{9,10},{10,1... | collective-permute-start | bytes 2359304 | tf_op jit(solution)/shard_map/ppermute | solution.py:24
  167.7 51.3 %collective-permute-start.2 = (bf16[1,768,512]{2,1,0:T(8,128)(2,1)}, bf16[1,768,512]{2,1,0:T(8,128)(2,1)S(1)}, u32[]{:S(2)}, u32[]{:S(2)}) collective-permute-start(bf16[1,768,512]{2,1,0:T(8,128)(2,1)} %collective-permute-done.1), channel_id=1, source_target_pairs={{0,1},{1,2},{2,3},{3,0},{4,5},{5,6},{6,7},{7,4},{8,9},{9,10},{10,1... | collective-permute-start | bytes 2359304 | tf_op jit(solution)/shard_map/ppermute | solution.py:24
  220.5 27.2 %all-to-all-start.1 = ((bf16[1,8,96,512]{3,2,0,1:T(8,128)(2,1)}), bf16[1,8,96,512]{3,2,0,1:T(8,128)(2,1)S(1)}, u32[]{:S(2)}, u32[]{:S(2)}) async-start(bf16[1,8,96,512]{3,2,0,1:T(8,128)(2,1)} %bitcast.117), calls=%async_computation.1 | async-start | bytes 1572864 | tf_op jit(solution)/shard_map/all_to_all | solution.py:61
  225.1 21.1 %collective-permute-start.5 = (bf16[1,768,512]{2,1,0:T(8,128)(2,1)}, bf16[1,768,512]{2,1,0:T(8,128)(2,1)S(1)}, u32[]{:S(2)}, u32[]{:S(2)}) collective-permute-start(bf16[1,768,512]{2,1,0:T(8,128)(2,1)} %collective-permute-done.4), channel_id=1, source_target_pairs={{0,1},{1,2},{2,3},{3,0},{4,5},{5,6},{6,7},{7,4},{8,9},{9,10},{10,1... | collective-permute-start | bytes 2359304 | tf_op jit(solution)/shard_map/ppermute | solution.py:24
  247.7 5.0 %copy-start.2 = (f32[256,4]{0,1:T(4,128)S(1)}, f32[256,4]{0,1:T(4,128)}, u32[]{:S(2)}) copy-start(f32[256,4]{0,1:T(4,128)} %param.10) | copy-start | bytes 12292
  247.7 25.8 %all-to-all-start.3 = ((bf16[1,8,96,512]{3,2,0,1:T(8,128)(2,1)}), bf16[1,8,96,512]{3,2,0,1:T(8,128)(2,1)S(1)}, u32[]{:S(2)}, u32[]{:S(2)}) async-start(bf16[1,8,96,512]{3,2,0,1:T(8,128)(2,1)} %bitcast.118), calls=%async_computation.3 | async-start | bytes 1572864 | tf_op jit(solution)/shard_map/all_to_all | solution.py:61
Sparse Core Ops, SparseCore 0:
  45.9 42.6 all-gather.2
  90.4 67.4 all-gather.4
